TPU v7x, 128 devices: a whole 4x4x4 slice. The times are simulated.
128 devices in a mesh: ep: 64 (over z, y, x), tp: 2 (over core).
Axes of the slice: x: 4, y: 4, z: 4, core: 2. Of those that a mesh axis runs over, the one named last changes fastest.
Arguments:
- residual: bfloat16 [1024, 4096], P(('ep', 'tp')), may hold values from -6 to 6
- lengths: int32 [1024], P(('ep', 'tp')), may hold values from 128 to 1024
- latent_cache: bfloat16 [1024, 1024, 512], P(('ep', 'tp'))
- rope_cache: bfloat16 [1024, 1024, 64], P(('ep', 'tp')), may hold values from -6 to 6
- route_ids: int32 [1024, 2], P(('ep', 'tp')), may hold values from 0 to 7, all different within a row; in each aligned block of 8 rows (0 to 7, 8 to 15, ...) at most 3 rows name the same one
- route_scores: bfloat16 [1024, 2], P(('ep', 'tp')), may hold values from -6 to 6
- norm_first: float32 [4096], replicated, may hold values from 0.1 to 1.9
- norm_second: float32 [4096], replicated, may hold values from 0.1 to 1.9
- query_gain: float32 [1024], replicated, may hold values from 0.1 to 1.9
- latent_gain: float32 [512], replicated, may hold values from 0.1 to 1.9
- query_down: bfloat16 [4096, 1024], P(('ep', 'tp')), may hold values from -0.09375 to 0.09375
- latent_down: bfloat16 [4096, 512], P(('ep', 'tp')), may hold values from -0.09375 to 0.09375
- rope_down: bfloat16 [4096, 64], replicated, may hold values from -0.09375 to 0.09375
- query_latent: bfloat16 [1024, 16384], P(None, ('ep', 'tp')), may hold values from -0.1875 to 0.1875
- query_rope: bfloat16 [1024, 2048], P(None, ('ep', 'tp')), may hold values from -0.1875 to 0.1875
- value_up: bfloat16 [512, 32, 128], replicated, may hold values from -1 to 1
- output_weight: bfloat16 [4096, 4096], P(None, ('ep', 'tp')), may hold values from -0.09375 to 0.09375
- expert_gate: bfloat16 [4096, 57344], P(None, ('ep', 'tp')), may hold values from -0.09375 to 0.09375
- expert_up: bfloat16 [4096, 57344], P(None, ('ep', 'tp')), may hold values from -0.09375 to 0.09375
- expert_down: bfloat16 [57344, 4096], P(('ep', 'tp')), may hold values from -0.125 to 0.125
Outputs:
- layer_out: bfloat16 [1024, 4096], P(('ep', 'tp'))
- new_latent: bfloat16 [1024, 512], P(('ep', 'tp'))
- new_rope: bfloat16 [1024, 64], P(('ep', 'tp'))
Inputs may be any that keep to these rules, and one draw needn't show every extreme that they name: `route_ids`: each row names 2 different experts. Within the rows of one device (aligned blocks of 8 rows) no expert is named more than 3 times; in every draw some expert is named exactly 3 times in some blocks. `lengths`: A sequence's cached positions are 0 to its length - 1; the new token stands at position length.
All inputs are finite; a program needn't handle non-finite values.
Results may differ from a plain program's by a relative error of at most 0.014.
The roundings to bfloat16 on the way count: a program that leaves them out, or rounds other values in their place, can miss the bound.
Values may be sent and summed in bfloat16 or wider, within the bound.
A program may use at most 128 MiB of HBM per device.

v0:
```python
import jax
import jax.numpy as jnp
from jax import lax
from jax.sharding import Mesh
from jax.sharding import PartitionSpec as P

ROPE = 64
NOPE = 128
EXPERTS = 8
TOP = 2
CAP = 3
EP_TP = ("ep_0", "ep_1", "ep_2", "tp")


epsilon = 1e-06
rope_base = 10000.0


def cut_along(shard, dim, peers):
    before, after = (shard.shape[:dim], shard.shape[dim + 1 :])
    return jnp.moveaxis(shard.reshape(*before, peers, -1, *after), dim, 0)


def sent_and_summed(shard, axis, dim):
    parts = cut_along(shard, dim, lax.axis_size(axis))
    arrived = lax.all_to_all(parts, axis, split_axis=0, concat_axis=0, tiled=True)
    return arrived.sum(axis=0)


def sum_by_axis(shard, axes, dim):
    far, near = axes
    parts = cut_along(shard, dim, lax.axis_size(far))
    nearer = sent_and_summed(parts, near, dim + 1)
    arrived = lax.all_to_all(nearer, far, split_axis=0, concat_axis=0, tiled=True)
    return arrived.sum(axis=0)


def sent_to_all(shard, axis):
    peers = lax.axis_size(axis)
    return lax.all_to_all(
        jnp.broadcast_to(shard[None], (peers, *shard.shape)), axis, 0, 0, tiled=True
    )


def in_order(parts, dim):
    shape = list(parts.shape[1:])
    shape[dim] *= parts.shape[0]
    return jnp.moveaxis(parts, 0, dim).reshape(shape)


def gathered_by_axis(shard, axes, dim):
    far, near = axes
    parts = sent_to_all(sent_to_all(shard, far), near)
    return in_order(parts.swapaxes(0, 1).reshape(-1, *shard.shape), dim)


def normalize(values_in, gain_row):
    return (
        values_in
        * lax.rsqrt(jnp.mean(values_in * values_in, axis=-1, keepdims=True) + epsilon)
        * gain_row
    )


def rotate(values_in, turns):
    half_width = values_in.shape[-1] // 2
    front_half = values_in[..., :half_width]
    back_half = values_in[..., half_width:]
    cosine = jnp.cos(turns)
    sine_part = jnp.sin(turns)
    return jnp.concatenate(
        [front_half * cosine - back_half * sine_part, front_half * sine_part + back_half * cosine],
        axis=-1,
    )


def rotary_angles(positions, rotary_width):
    inverse = rope_base ** (-jnp.arange(0, rotary_width, 2, dtype=jnp.float32) / rotary_width)
    return positions.astype(jnp.float32)[:, None] * inverse[None, :]


def slot_tables(route_block):
    experts = jnp.arange(EXPERTS, dtype=jnp.int32)
    onehot = (route_block[..., None] == experts).astype(jnp.int32)
    earlier = jnp.cumsum(onehot, axis=-2) - onehot
    slot_rank = jnp.sum(earlier * onehot, axis=-1)
    places = jnp.arange(CAP, dtype=jnp.int32)
    return onehot[..., None] * (slot_rank[..., None, None] == places).astype(jnp.int32)


def owner_table(sequences):
    assign = sequences * TOP
    return (
        jnp.arange(assign, dtype=jnp.int32)[None, :] // TOP
        == jnp.arange(sequences, dtype=jnp.int32)[:, None]
    ).astype(jnp.float32)


def expert_rows(row_block, expert_gate, expert_up, expert_down):
    gate_part = jnp.dot(row_block, expert_gate, preferred_element_type=jnp.float32)
    up_part = jnp.dot(row_block, expert_up, preferred_element_type=jnp.float32)
    hidden = (jax.nn.silu(gate_part) * up_part).astype(jnp.bfloat16)
    return jnp.dot(hidden, expert_down, preferred_element_type=jnp.float32)


def attend_local(
    query_latents, query_rotary, latent_cache, rope_cache, new_latent, new_rope, lengths
):
    score_scale = (NOPE + ROPE) ** (-0.5)
    cache_scores = (
        jnp.einsum("shl,spl->shp", query_latents, latent_cache, preferred_element_type=jnp.float32)
        + jnp.einsum("shr,spr->shp", query_rotary, rope_cache, preferred_element_type=jnp.float32)
    ) * score_scale
    new_scores = (
        jnp.einsum("shl,sl->sh", query_latents, new_latent, preferred_element_type=jnp.float32)
        + jnp.einsum("shr,sr->sh", query_rotary, new_rope, preferred_element_type=jnp.float32)
    ) * score_scale
    visible = jnp.arange(latent_cache.shape[1], dtype=jnp.int32)[None, :] < lengths[:, None]
    cache_scores = jnp.where(visible[:, None, :], cache_scores, -jnp.inf)
    row_top = jnp.maximum(jnp.max(cache_scores, axis=-1), new_scores)
    cache_terms = jnp.exp(cache_scores - row_top[..., None])
    new_term = jnp.exp(new_scores - row_top)
    denominator = jnp.sum(cache_terms, axis=-1) + new_term
    cache_probs = (cache_terms / denominator[..., None]).astype(jnp.bfloat16)
    new_probs = (new_term / denominator).astype(jnp.bfloat16)
    mixture = jnp.einsum(
        "shp,spl->shl", cache_probs, latent_cache, preferred_element_type=jnp.float32
    )
    mixture = (
        mixture
        + new_probs.astype(jnp.float32)[..., None] * new_latent.astype(jnp.float32)[:, None, :]
    )
    return mixture.astype(jnp.bfloat16)


def local(
    residual,
    lengths,
    latent_cache,
    rope_cache,
    route_ids,
    route_scores,
    norm_first,
    norm_second,
    query_gain,
    latent_gain,
    query_down,
    latent_down,
    rope_down,
    query_latent,
    query_rope,
    value_up,
    output_weight,
    expert_gate,
    expert_up,
    expert_down,
):
    sequences = residual.shape[0]
    model_width = residual.shape[1]
    devices = lax.axis_size(EP_TP)
    stream = residual.astype(jnp.float32)
    normed = normalize(stream, norm_first).astype(jnp.bfloat16)
    slices = lax.all_to_all(normed, EP_TP, split_axis=1, concat_axis=0, tiled=True)
    query_width = query_down.shape[1]
    lowered = sum_by_axis(
        jnp.concatenate(
            [
                jnp.dot(slices, query_down, preferred_element_type=jnp.float32),
                jnp.dot(slices, latent_down, preferred_element_type=jnp.float32),
            ],
            axis=1,
        ),
        (("ep_0", "ep_1", "ep_2"), "tp"),
        0,
    )
    query_small = normalize(lowered[:, :query_width], query_gain).astype(jnp.bfloat16)
    new_latent = normalize(lowered[:, query_width:], latent_gain).astype(jnp.bfloat16)
    turns = rotary_angles(lengths, rope_down.shape[1])
    new_rope = rotate(jnp.dot(normed, rope_down, preferred_element_type=jnp.float32), turns).astype(
        jnp.bfloat16
    )
    latent_columns = query_latent.shape[1]
    shard_rows = gathered_by_axis(query_small, (("ep_0", "ep_1", "ep_2"), "tp"), 0)
    columns = jnp.concatenate(
        [
            jnp.dot(shard_rows, query_latent, preferred_element_type=jnp.float32),
            jnp.dot(shard_rows, query_rope, preferred_element_type=jnp.float32),
        ],
        axis=1,
    ).astype(jnp.bfloat16)
    at_home = lax.all_to_all(columns, EP_TP, split_axis=0, concat_axis=1, tiled=True)
    at_home = at_home.reshape(sequences, devices, columns.shape[1])
    head_count = value_up.shape[1]
    query_latents = at_home[:, :, :latent_columns].reshape(sequences, head_count, -1)
    query_pe = at_home[:, :, latent_columns:].reshape(sequences, head_count, -1)
    query_rotary = rotate(query_pe.astype(jnp.float32), turns[:, None, :]).astype(jnp.bfloat16)
    mixture = attend_local(
        query_latents, query_rotary, latent_cache, rope_cache, new_latent, new_rope, lengths
    )
    values = jnp.einsum("shl,lhv->shv", mixture, value_up, preferred_element_type=jnp.float32)
    values = values.astype(jnp.bfloat16).reshape(sequences, -1)
    output_cols = jnp.dot(
        lax.all_gather(values, EP_TP, axis=0, tiled=True),
        output_weight,
        preferred_element_type=jnp.float32,
    ).astype(jnp.bfloat16)
    attended = lax.all_to_all(output_cols, EP_TP, split_axis=0, concat_axis=1, tiled=True)
    after_attention = stream + attended.astype(jnp.float32)
    second = normalize(after_attention, norm_second).astype(jnp.bfloat16)
    owners = owner_table(sequences)
    assign = sequences * TOP
    group_size = devices // EXPERTS
    weights = jax.nn.softmax(route_scores.astype(jnp.float32), axis=-1)
    matches = slot_tables(route_ids.reshape(1, assign))[0].astype(jnp.float32)
    picker = jnp.einsum("aec,sa->ecs", matches, owners).astype(jnp.bfloat16)
    outbound = jnp.einsum("ecs,sd->ecd", picker, second, preferred_element_type=jnp.float32).astype(
        jnp.bfloat16
    )
    outbound = jnp.broadcast_to(outbound[:, None], (EXPERTS, group_size, CAP, model_width))
    outbound = outbound.reshape(devices, CAP, model_width)
    arrived = lax.all_to_all(outbound, EP_TP, split_axis=0, concat_axis=0, tiled=True)
    partial_value = expert_rows(
        arrived.reshape(-1, model_width), expert_gate, expert_up, expert_down
    )
    returned = lax.all_to_all(
        partial_value.reshape(arrived.shape).astype(jnp.bfloat16),
        EP_TP,
        split_axis=0,
        concat_axis=0,
        tiled=True,
    ).astype(jnp.float32)
    summed = jnp.sum(returned.reshape(EXPERTS, group_size, CAP, model_width), axis=1)
    combine_weights = matches * weights.reshape(assign)[:, None, None]
    token_weights = jnp.einsum("aec,sa->sec", combine_weights, owners)
    routed = jnp.einsum("sec,ecd->sd", token_weights, summed)
    layer_out = (after_attention + routed).astype(jnp.bfloat16)
    return (layer_out, new_latent, new_rope)


def solution(mesh):
    torus = Mesh(mesh.devices.reshape(4, 4, 4, mesh.shape["tp"]), ("ep_0", "ep_1", "ep_2", "tp"))
    placed = (
        P(EP_TP, None),
        P(EP_TP),
        P(EP_TP, None, None),
        P(EP_TP, None, None),
        P(EP_TP, None),
        P(EP_TP, None),
        P(),
        P(),
        P(),
        P(),
        P(EP_TP, None),
        P(EP_TP, None),
        P(),
        P(None, EP_TP),
        P(None, EP_TP),
        P(),
        P(None, EP_TP),
        P(None, EP_TP),
        P(None, EP_TP),
        P(EP_TP, None),
    )
    return jax.shard_map(
        local,
        mesh=torus,
        in_specs=placed,
        out_specs=(P(EP_TP, None), P(EP_TP, None), P(EP_TP, None)),
        check_vma=False,
    )
```

profile of v0, /device:TPU:1, one launch (start us, length us, event | category | flops | bytes accessed | tf_op | source)
XLA Modules:
  0.0 437.4 jit_solution(7753741035902536983)
XLA Ops:
  7.2 1.1 fusion.27
  8.3 0.9 fusion.29
  9.2 0.2 all_to_all.52
  9.4 0.2 copy.115
  9.6 0.2 reshape.366
  9.8 20.9 %all_to_all.75 = bf16[128,2,128]{2,1,0:T(2,128)(2,1)S(1)} all-to-all(bf16[128,2,128]{2,1,0:T(2,128)(2,1)S(1)} %reshape.366), channel_id=1, replica_groups=mesh['ep_0'=4,'ep_1'=4,'ep_2'=4,'tp'=2] {'ep_0','ep_1','ep_2','tp'}, dimensions={0} | all-to-all | bytes 131072 | tf_op jit(solution)/shard_map/all_to_all | solution.py:163
  30.7 0.2 reshape.367
  30.9 1.2 fusion.22
  32.1 0.8 fusion.24
  32.9 3.2 pad_maximum_fusion
  36.1 6.5 %copy.77 = f32[1024,1536]{1,0:T(8,128)} copy(f32[1024,1536]{0,1:T(8,128)} %pad_maximum_fusion) | data formatting | bytes 12582912 | tf_op jit(solution)/shard_map/concatenate | solution.py:166
  42.6 3.2 copy.78
  45.9 10.4 %all_to_all.76 = f32[2,64,8,1536]{3,2,1,0:T(8,128)} all-to-all(f32[2,64,8,1536]{3,2,1,0:T(8,128)S(1)} %copy.78), channel_id=1, replica_groups=mesh['ep_0'=4,'ep_1'=4,'ep_2'=4,'tp'=2] {'tp'}, dimensions={0} | all-to-all | bytes 12582912 | tf_op jit(solution)/shard_map/all_to_all | solution.py:26
  56.2 5.4 %reduce_sum.91 = f32[64,8,1536]{2,1,0:T(8,128)} reduce(f32[2,64,8,1536]{3,2,1,0:T(8,128)} %all_to_all.76, f32[]{:T(128)} %constant.38.clone.1), dimensions={0}, to_apply=%region_1.0 | reduce | flops 786432 | bytes 9437188 | tf_op jit(solution)/shard_map/reduce_sum | solution.py:27
  61.6 46.3 %all_to_all.77 = f32[64,8,1536]{2,1,0:T(8,128)} all-to-all(f32[64,8,1536]{2,1,0:T(8,128)} %reduce_sum.91), channel_id=1, replica_groups=mesh['ep_0'=4,'ep_1'=4,'ep_2'=4,'tp'=2] {'ep_0','ep_1','ep_2'}, dimensions={0} | all-to-all | bytes 6291456 | tf_op jit(solution)/shard_map/all_to_all | solution.py:34
  108.0 2.1 reduce_sum.92
  110.3 1.1 broadcast_in_dim.15
  111.4 5.7 %all-to-all-start.3 = ((bf16[64,8,1024]{2,1,0:T(8,128)(2,1)}), bf16[64,8,1024]{2,1,0:T(8,128)(2,1)S(1)}, u32[]{:S(2)}, u32[]{:S(2)}) async-start(bf16[64,8,1024]{2,1,0:T(8,128)(2,1)} %broadcast_in_dim.15), calls=%async_computation.3 | async-start | bytes 2097152 | tf_op jit(solution)/shard_map/all_to_all | solution.py:40
  117.2 0.2 fusion.84
  117.8 17.4 %all-to-all-done.3 = bf16[64,8,1024]{2,1,0:T(8,128)(2,1)S(1)} async-done(((bf16[64,8,1024]{2,1,0:T(8,128)(2,1)}), bf16[64,8,1024]{2,1,0:T(8,128)(2,1)S(1)}, u32[]{:S(2)}, u32[]{:S(2)}) %all-to-all-start.3) | async-done | bytes 1048608 | tf_op jit(solution)/shard_map/all_to_all | solution.py:40
  135.2 0.6 copy.79
  135.8 0.3 broadcast_in_dim.16
  136.0 6.9 %all_to_all.78 = bf16[2,64,8,1024]{3,1,2,0:T(8,128)(2,1)S(1)} all-to-all(bf16[2,64,8,1024]{3,1,2,0:T(8,128)(2,1)S(1)} %broadcast_in_dim.16), channel_id=1, replica_groups=mesh['ep_0'=4,'ep_1'=4,'ep_2'=4,'tp'=2] {'tp'}, dimensions={0} | all-to-all | bytes 4194304 | tf_op jit(solution)/shard_map/all_to_all | solution.py:40
  142.9 3.5 copy.80
  146.4 2.8 dot_general.61
  149.3 0.6 convolution_convert_fusion.4
  149.9 0.8 convolution_convert_fusion.2
  150.8 1.2 copy.82
  152.0 3.7 all-to-all-start.5
  155.9 13.6 %all-to-all-done.5 = bf16[128,8,144]{2,1,0:T(8,128)(2,1)S(1)} async-done(((bf16[128,8,144]{2,1,0:T(8,128)(2,1)}), bf16[128,8,144]{2,1,0:T(8,128)(2,1)S(1)}, u32[]{:S(2)}, u32[]{:S(2)}) %all-to-all-start.5) | async-done | bytes 294944 | tf_op jit(solution)/shard_map/all_to_all | solution.py:191
  169.4 0.4 copy.83
  169.9 0.2 copy.84
  170.1 0.2 reshape.347
  170.3 0.2 copy.85
  170.5 0.2 reshape.353
  170.6 0.2 fusion.35
  170.8 5.9 %fusion.83 = f32[8,32,1024]{2,1,0:T(8,128)S(1)} fusion(bf16[8,32,512]{2,1,0:T(8,128)(2,1)S(1)} %reshape.347, bf16[8,1024,512]{2,1,0:T(8,128)(2,1)} %param.22), kind=kOutput, calls=%fused_computation.115 | convolution fusion | flops 268435456 | bytes 9699328 | tf_op jit(solution)/shard_map/shl,spl->shp/dot_general | solution.py:111
  176.9 0.2 fusion.47
  177.1 0.5 fusion.80
  177.6 0.3 fusion.16
  177.9 5.2 %fusion.7 = bf16[8,32,512]{2,1,0:T(8,128)(2,1)S(1)} fusion(bf16[8,1024,512]{2,1,0:T(8,128)(2,1)} %param.22, f32[8,32,1024]{2,1,0:T(8,128)S(1)} %get-tuple-element.14, f32[8,32]{1,0:T(8,128)S(1)} %get-tuple-element.8, f32[8,32]{1,0:T(8,128)S(1)} %fusion.72, f32[8,512]{1,0:T(8,128)S(1)} %get-tuple-element.3, f32[8,32]{1,0:T(8,128)S(1)} %get-tuple-element.7), kind=kOutput, calls=%fused_computation.15 | convolution fusion | flops 269615104 | bytes 9718784 | tf_op jit(solution)/shard_map/shp,spl->shl/dot_general | solution.py:126
  183.1 5.2 %fusion.11 = bf16[8,4096]{1,0:T(8,128)(2,1)} fusion(bf16[512,32,128]{2,1,0:T(8,128)(2,1)S(1)} %copy-done.2, bf16[8,32,512]{2,1,0:T(8,128)(2,1)S(1)} %fusion.7), kind=kOutput, calls=%fused_computation.18 | convolution fusion | flops 33587200 | bytes 4521984 | tf_op jit(solution)/shard_map/shl,lhv->shv/dot_general | solution.py:200
  188.7 0.2 select_reduce_fusion
  188.9 66.1 %all-gather.2.cloned.1.call-done = bf16[1024,4096]{1,0:T(8,128)(2,1)} async-done(((bf16[8,4096]{1,0:T(8,128)(2,1)}), bf16[1024,4096]{1,0:T(8,128)(2,1)}) %all-gather.2.cloned.1.call-update) | async-done | bytes 8388624 | tf_op jit(solution)/shard_map/all_gather | solution.py:203
  254.9 5.9 %convolution_convert_fusion.3 = bf16[1024,32]{0,1:T(8,128)(2,1)S(1)} fusion(bf16[1024,4096]{1,0:T(8,128)(2,1)} %all-gather.2.cloned.1.call-done, bf16[4096,32]{0,1:T(8,128)(2,1)S(1)} %copy-done.6), kind=kOutput, calls=%fused_computation.19 | convolution fusion | flops 268468224 | bytes 8716288 | tf_op jit(solution)/shard_map/dot_general | solution.py:202
  260.9 0.2 copy.88
  261.1 0.8 reshape.368
  261.9 5.4 %all-to-all-start.6 = ((bf16[128,2,128]{2,1,0:T(2,128)(2,1)}), bf16[128,2,128]{2,1,0:T(2,128)(2,1)S(1)}, u32[]{:S(2)}, u32[]{:S(2)}) async-start(bf16[128,2,128]{2,1,0:T(2,128)(2,1)} %reshape.368), calls=%async_computation.6 | async-start | bytes 131072 | tf_op jit(solution)/shard_map/all_to_all | solution.py:207
  267.3 9.5 %all-to-all-done.6 = bf16[128,2,128]{2,1,0:T(2,128)(2,1)S(1)} async-done(((bf16[128,2,128]{2,1,0:T(2,128)(2,1)}), bf16[128,2,128]{2,1,0:T(2,128)(2,1)S(1)}, u32[]{:S(2)}, u32[]{:S(2)}) %all-to-all-start.6) | async-done | bytes 65568 | tf_op jit(solution)/shard_map/all_to_all | solution.py:207
  276.8 0.2 reshape.369
  277.1 0.2 reshape.354
  277.6 0.3 convolution_convert_fusion.1
  277.9 0.2 copy.92
  278.1 2.1 broadcast_in_dim.18
  280.2 57.3 %all_to_all.79 = bf16[128,3,4096]{2,1,0:T(4,128)(2,1)} all-to-all(bf16[128,3,4096]{2,1,0:T(4,128)(2,1)S(1)} %bitcast.84), channel_id=1, replica_groups=mesh['ep_0'=4,'ep_1'=4,'ep_2'=4,'tp'=2] {'ep_0','ep_1','ep_2','tp'}, dimensions={0} | all-to-all | bytes 6291456 | tf_op jit(solution)/shard_map/all_to_all | solution.py:221
  337.5 7.4 %reshape.350 = bf16[384,4096]{1,0:T(8,128)(2,1)} reshape(bf16[128,3,4096]{2,1,0:T(4,128)(2,1)} %all_to_all.79) | data formatting | bytes 6291456 | tf_op jit(solution)/shard_map/reshape | solution.py:223
  344.9 5.1 %fusion.85 = f32[384,448]{0,1:T(8,128)S(1)} fusion(bf16[384,4096]{1,0:T(8,128)(2,1)} %reshape.350, bf16[4096,448]{0,1:T(8,128)(2,1)} %param.37), kind=kOutput, calls=%fused_computation.117 | convolution fusion | flops 1409286144 | bytes 7503872 | tf_op jit(solution)/shard_map/dot_general | solution.py:100
  350.0 9.6 %convolution_convert_fusion = bf16[384,4096]{1,0:T(8,128)(2,1)} fusion(bf16[448,4096]{1,0:T(8,128)(2,1)} %param.39, bf16[384,4096]{1,0:T(8,128)(2,1)} %reshape.350, bf16[4096,448]{0,1:T(8,128)(2,1)} %param.38, f32[384,448]{0,1:T(8,128)S(1)} %fusion.85), kind=kOutput, calls=%fused_computation.2 | convolution fusion | flops 2821177344 | bytes 14319616 | tf_op jit(solution)/shard_map/dot_general | solution.py:103
  359.6 7.1 %convert_element_type.144 = bf16[128,3,4096]{2,1,0:T(4,128)(2,1)} reshape(bf16[384,4096]{1,0:T(8,128)(2,1)} %convolution_convert_fusion) | data formatting | bytes 6291456 | tf_op jit(solution)/shard_map/convert_element_type | solution.py:226
  366.7 5.6 %all-to-all-start.8 = ((bf16[128,3,4096]{2,1,0:T(4,128)(2,1)}), bf16[128,3,4096]{2,1,0:T(4,128)(2,1)}, u32[]{:S(2)}, u32[]{:S(2)}) async-start(bf16[128,3,4096]{2,1,0:T(4,128)(2,1)} %convert_element_type.144), calls=%async_computation.8 | async-start | bytes 8388608 | tf_op jit(solution)/shard_map/all_to_all | solution.py:225
  372.6 0.7 pad_maximum_fusion.5
  373.3 51.8 %all-to-all-done.8 = bf16[128,3,4096]{2,1,0:T(4,128)(2,1)} async-done(((bf16[128,3,4096]{2,1,0:T(4,128)(2,1)}), bf16[128,3,4096]{2,1,0:T(4,128)(2,1)}, u32[]{:S(2)}, u32[]{:S(2)}) %all-to-all-start.8) | async-done | bytes 3145760 | tf_op jit(solution)/shard_map/all_to_all | solution.py:225
  425.1 4.4 %convert_reduce_fusion = bf16[8,3,4096]{2,1,0:T(4,128)(2,1)S(1)} fusion(bf16[128,3,4096]{2,1,0:T(4,128)(2,1)} %all-to-all-done.8), kind=kLoop, calls=%fused_computation | loop fusion | flops 3047424 | bytes 3342336 | tf_op jit(solution)/shard_map/reduce_sum | solution.py:232
  429.5 1.0 fusion.1
  (69 shorter events, 1.9 us)
Async XLA Ops:
  7.2 169.9 %copy-start = (bf16[8,1024,64]{1,2,0:T(8,128)(2,1)S(1)}, bf16[8,1024,64]{1,2,0:T(8,128)(2,1)}, u32[]{:S(2)}) copy-start(bf16[8,1024,64]{1,2,0:T(8,128)(2,1)} %param.23) | copy-start | bytes 3145732
  7.2 24.9 %copy-start.7 = (bf16[32,1024]{1,0:T(8,128)(2,1)S(1)}, bf16[32,1024]{1,0:T(8,128)(2,1)}, u32[]{:S(2)}) copy-start(bf16[32,1024]{1,0:T(8,128)(2,1)} %param.30) | copy-start | bytes 196612
  61.6 48.6 %copy-start.11 = (f32[1024]{0:T(1024)S(1)}, f32[1024]{0:T(1024)}, u32[]{:S(2)}) copy-start(f32[1024]{0:T(1024)} %param.28) | copy-start | bytes 12292
  107.9 9.2 %copy-start.14 = (s32[8]{0:T(128)S(1)}, s32[8]{0:T(128)}, u32[]{:S(2)}) copy-start(s32[8]{0:T(128)} %param.21) | copy-start | bytes 100
  108.0 9.2 %copy-start.4 = (bf16[4096,64]{0,1:T(8,128)(2,1)S(1)}, bf16[4096,64]{0,1:T(8,128)(2,1)}, u32[]{:S(2)}) copy-start(bf16[4096,64]{0,1:T(8,128)(2,1)} %param.32) | copy-start | bytes 1572868
  111.4 23.8 %all-to-all-start.3 = ((bf16[64,8,1024]{2,1,0:T(8,128)(2,1)}), bf16[64,8,1024]{2,1,0:T(8,128)(2,1)S(1)}, u32[]{:S(2)}, u32[]{:S(2)}) async-start(bf16[64,8,1024]{2,1,0:T(8,128)(2,1)} %broadcast_in_dim.15), calls=%async_computation.3 | async-start | bytes 2097152 | tf_op jit(solution)/shard_map/all_to_all | solution.py:40
  142.9 6.3 %copy-start.8 = (bf16[1024,16]{0,1:T(8,128)(2,1)S(1)}, bf16[1024,16]{0,1:T(8,128)(2,1)}, u32[]{:S(2)}) copy-start(bf16[1024,16]{0,1:T(8,128)(2,1)} %param.34) | copy-start | bytes 98308
  146.4 3.5 copy-start.5
  149.2 6.5 %copy-start.12 = (f32[512]{0:T(512)S(1)}, f32[512]{0:T(512)}, u32[]{:S(2)}) copy-start(f32[512]{0:T(512)} %param.29) | copy-start | bytes 6148
  152.0 17.5 %all-to-all-start.5 = ((bf16[128,8,144]{2,1,0:T(8,128)(2,1)}), bf16[128,8,144]{2,1,0:T(8,128)(2,1)S(1)}, u32[]{:S(2)}, u32[]{:S(2)}) async-start(bf16[128,8,144]{2,1,0:T(8,128)(2,1)} %copy.82), calls=%async_computation.5 | async-start | bytes 1048576 | tf_op jit(solution)/shard_map/all_to_all | solution.py:191
  155.7 99.2 %all-gather.2.cloned.1.call-start = ((), (), s32[]{:S(2)}) async-start(), calls=%async_computation.9 | async-start | bytes 8454144 | tf_op jit(solution)/shard_map/all_gather | solution.py:203
  155.8 20.9 %copy-start.10 = (bf16[8,512]{1,0:T(8,128)(2,1)}, bf16[8,512]{1,0:T(8,128)(2,1)S(1)}, u32[]{:S(2)}) copy-start(bf16[8,512]{1,0:T(8,128)(2,1)S(1)} %get-tuple-element.4) | copy-start | bytes 24580
  177.9 5.2 %copy-start.2 = (bf16[512,32,128]{2,1,0:T(8,128)(2,1)S(1)}, bf16[512,32,128]{2,1,0:T(8,128)(2,1)}, u32[]{:S(2)}) copy-start(bf16[512,32,128]{2,1,0:T(8,128)(2,1)} %param.35) | copy-start | bytes 12582916
  183.1 5.3 %copy-start.13 = (s32[8,2]{0,1:T(2,128)S(1)}, s32[8,2]{0,1:T(2,128)}, u32[]{:S(2)}) copy-start(s32[8,2]{0,1:T(2,128)} %param.24) | copy-start | bytes 196
  183.1 71.8 %copy-start.6 = (bf16[4096,32]{0,1:T(8,128)(2,1)S(1)}, bf16[4096,32]{0,1:T(8,128)(2,1)}, u32[]{:S(2)}) copy-start(bf16[4096,32]{0,1:T(8,128)(2,1)} %param.36) | copy-start | bytes 786436
  188.9 88.5 %copy-start.3 = (bf16[8,4096]{1,0:T(8,128)(2,1)S(1)}, bf16[8,4096]{1,0:T(8,128)(2,1)}, u32[]{:S(2)}) copy-start(bf16[8,4096]{1,0:T(8,128)(2,1)} %param.20) | copy-start | bytes 196612
  260.9 16.7 %copy-start.9 = (f32[4096]{0:T(1024)S(1)}, f32[4096]{0:T(1024)}, u32[]{:S(2)}) copy-start(f32[4096]{0:T(1024)} %param.27) | copy-start | bytes 49156
  261.9 14.9 %all-to-all-start.6 = ((bf16[128,2,128]{2,1,0:T(2,128)(2,1)}), bf16[128,2,128]{2,1,0:T(2,128)(2,1)S(1)}, u32[]{:S(2)}, u32[]{:S(2)}) async-start(bf16[128,2,128]{2,1,0:T(2,128)(2,1)} %reshape.368), calls=%async_computation.6 | async-start | bytes 131072 | tf_op jit(solution)/shard_map/all_to_all | solution.py:207
  366.7 5.7 %copy-start.15 = (bf16[8,2]{0,1:T(2,128)(2,1)S(1)}, bf16[8,2]{0,1:T(2,128)(2,1)}, u32[]{:S(2)}) copy-start(bf16[8,2]{0,1:T(2,128)(2,1)} %param.25) | copy-start | bytes 100
  366.7 58.4 %all-to-all-start.8 = ((bf16[128,3,4096]{2,1,0:T(4,128)(2,1)}), bf16[128,3,4096]{2,1,0:T(4,128)(2,1)}, u32[]{:S(2)}, u32[]{:S(2)}) async-start(bf16[128,3,4096]{2,1,0:T(4,128)(2,1)} %convert_element_type.144), calls=%async_computation.8 | async-start | bytes 8388608 | tf_op jit(solution)/shard_map/all_to_all | solution.py:225
  372.4 58.2 %copy-start.1 = (bf16[8,1024,64]{1,2,0:T(8,128)(2,1)S(1)}, bf16[8,1024,64]{1,2,0:T(8,128)(2,1)}, u32[]{:S(2)}) copy-start(bf16[8,1024,64]{1,2,0:T(8,128)(2,1)} %param.23) | copy-start | bytes 3145732
Sparse Core Ops, SparseCore 0:
  188.5 66.3 all-gather.1
where the time goes:
time: 439 us; the launch traced here: 437 us
  waiting for transfers between devices  158 us (36%)
  blocking collectives  142 us (32%)
  matrix products  42.9 us (10%)
  local copies, waits for them, and re-layouts  39.7 us (9%)
  starting transfers between devices  20.5 us (5%)
  other arithmetic  19.6 us (4%)
  between operations  14.5 us (3%)
    all_gather x1, waiting for transfers between devices, local(): lax.all_gather(values, EP_TP, axis=0, tiled=True)  66.1 us
    all_to_all x1, blocking collectives, local(): lax.all_to_all(outbound, EP_TP, split_axis=0, concat_axis=0, tiled=True)  57.3 us
    all_to_all x1, waiting for transfers between devices, local(): lax.all_to_all(partial_value.reshape(arrived.shape).astype(jnp.bfloat16),...  51.8 us
    all_to_all x1, blocking collectives, sum_by_axis(): lax.all_to_all(nearer, far, split_axis=0, concat_axis=0, tiled=True)  46.3 us
    all_to_all x1, blocking collectives, local(): lax.all_to_all(normed, EP_TP, split_axis=1, concat_axis=0, tiled=True)  20.9 us
    all_to_all x1, waiting for transfers between devices, sent_to_all(): lax.all_to_all(jnp.broadcast_to(shard[None], (peers, *shard.shape)), axis...  17.4 us
    all_to_all x1, waiting for transfers between devices, local(): lax.all_to_all(columns, EP_TP, split_axis=0, concat_axis=1, tiled=True)  13.6 us
    all_to_all x1, blocking collectives, sent_and_summed(): lax.all_to_all(parts, axis, split_axis=0, concat_axis=0, tiled=True)  10.4 us
  transfers between devices with their start and end apart: 5, of which 5 were waited for; matrix products, arithmetic and copies ran while one was open for 0% of the time, Pallas kernels for 0%

commit v1 on v0

--- a/solution.py
+++ b/solution.py
@@ -1,6 +1,8 @@
 import jax
 import jax.numpy as jnp
 from jax import lax
+from jax.experimental import pallas as pl
+from jax.experimental.pallas import tpu as pltpu
 from jax.sharding import Mesh
 from jax.sharding import PartitionSpec as P
 
@@ -10,6 +12,10 @@
 TOP = 2
 CAP = 3
 EP_TP = ("ep_0", "ep_1", "ep_2", "tp")
+MESH = pl.DeviceIdType.MESH
+HID = 448
+F32 = jnp.float32
+BF16 = jnp.bfloat16
 
 
 epsilon = 1e-06
@@ -96,11 +102,217 @@
     ).astype(jnp.float32)
 
 
-def expert_rows(row_block, expert_gate, expert_up, expert_down):
-    gate_part = jnp.dot(row_block, expert_gate, preferred_element_type=jnp.float32)
-    up_part = jnp.dot(row_block, expert_up, preferred_element_type=jnp.float32)
-    hidden = (jax.nn.silu(gate_part) * up_part).astype(jnp.bfloat16)
-    return jnp.dot(hidden, expert_down, preferred_element_type=jnp.float32)
+def here():
+    return tuple(lax.axis_index(name) for name in EP_TP)
+
+
+def ring_peer(step, z, y, x):
+    return (z + step // 16) % 4, (y + (step // 4) % 4) % 4, (x + step % 4) % 4
+
+
+def block_wait(ref, count, sem, device):
+    return pltpu.make_async_remote_copy(
+        src_ref=ref.at[pl.ds(0, count)],
+        dst_ref=ref.at[pl.ds(0, count)],
+        send_sem=sem,
+        recv_sem=sem,
+        device_id=device,
+        device_id_type=MESH,
+    )
+
+
+def expert_kernel(
+    blocks,
+    mixer,
+    after,
+    gate_hbm,
+    up_hbm,
+    down_hbm,
+    out,
+    gate,
+    up,
+    down,
+    arrived,
+    wide,
+    rows,
+    hidden,
+    leaving,
+    returned,
+    summed,
+    load_sem,
+    swap_send,
+    swap_recv,
+    out_send,
+    out_recv,
+    back_send,
+    back_recv,
+):
+    z, y, x, c = here()
+    me = (z * 4 + y) * 4 + x
+    mine = pl.ds(pl.multiple_of(c * HID, 64), HID)
+    weights = ((gate_hbm, gate), (up_hbm, up), (down_hbm, down))
+    loads = [
+        pltpu.make_async_copy(src, dst.at[mine], load_sem.at[i])
+        for i, (src, dst) in enumerate(weights)
+    ]
+    for load in loads:
+        load.start()
+    twin = (z, y, x, 1 - c)
+    barrier = pltpu.get_barrier_semaphore()
+
+    def greet(step, carry):
+        pz, py, px = ring_peer(step, z, y, x)
+        pl.semaphore_signal(barrier, inc=1, device_id=(pz, py, px, c), device_id_type=MESH)
+        return carry
+
+    lax.fori_loop(1, 64, greet, 0)
+    pl.semaphore_signal(barrier, inc=1, device_id=twin, device_id_type=MESH)
+    pl.semaphore_wait(barrier, 64)
+
+    def dispatch(step, carry):
+        pz, py, px = ring_peer(step, z, y, x)
+        pltpu.make_async_remote_copy(
+            src_ref=blocks.at[2 * pz + py // 2],
+            dst_ref=arrived.at[me],
+            send_sem=out_send,
+            recv_sem=out_recv,
+            device_id=(pz, py, px, c),
+            device_id_type=MESH,
+        ).start()
+        return carry
+
+    lax.fori_loop(1, 64, dispatch, 0)
+    swaps = [
+        pltpu.make_async_remote_copy(
+            src_ref=src,
+            dst_ref=dst.at[mine],
+            send_sem=swap_send.at[i],
+            recv_sem=swap_recv.at[i],
+            device_id=twin,
+            device_id_type=MESH,
+        )
+        for i, (src, dst) in enumerate(weights)
+    ]
+    for swap in swaps:
+        swap.start()
+    arrived[me] = blocks[2 * z + y // 2]
+    for load in loads:
+        load.wait()
+    block_wait(arrived, 63, out_recv, twin).wait_recv()
+
+    def widen(s, carry):
+        block = arrived[s].astype(F32)
+        at = pl.ds(pl.multiple_of(s * 24, 8), 24)
+        for j in range(4):
+            wide[j, at, :] = block[:, j * 128 : (j + 1) * 128]
+        return carry
+
+    lax.fori_loop(0, 64, widen, 0)
+    for q in range(8):
+        for j in range(4):
+            lane = q * 512 + j * 128
+            rows[:, lane : lane + 128] = wide[j, pl.ds(q, 192, stride=8), :].astype(BF16)
+    swaps[0].wait_recv()
+    swaps[1].wait_recv()
+
+    nt = (((1,), (1,)), ((), ()))
+
+    def lift(half, carry):
+        at = pl.ds(pl.multiple_of(half * HID, 64), HID)
+        gated = lax.dot_general(rows[...], gate[at, :], nt, preferred_element_type=F32)
+        upped = lax.dot_general(rows[...], up[at, :], nt, preferred_element_type=F32)
+        hidden[half] = (jax.nn.silu(gated) * upped).astype(BF16)
+        return carry
+
+    lax.fori_loop(0, 2, lift, 0)
+    swaps[2].wait_recv()
+
+    def lower(q, carry):
+        at = pl.ds(pl.multiple_of(q * 512, 512), 512)
+        part = jnp.dot(hidden[0], down[0:HID, at], preferred_element_type=F32)
+        part += jnp.dot(hidden[1], down[HID : 2 * HID, at], preferred_element_type=F32)
+        for j in range(4):
+            wide[j, pl.ds(q, 192, stride=8), :] = part[:, j * 128 : (j + 1) * 128]
+        return carry
+
+    lax.fori_loop(0, 8, lower, 0)
+
+    def narrow(s, carry):
+        at = pl.ds(pl.multiple_of(s * 24, 8), 24)
+        leaving[s] = jnp.concatenate([wide[j, at, :] for j in range(4)], axis=1).astype(BF16)
+        return carry
+
+    lax.fori_loop(0, 64, narrow, 0)
+
+    def give_back(step, carry):
+        pz, py, px = ring_peer(step, z, y, x)
+        pltpu.make_async_remote_copy(
+            src_ref=leaving.at[(pz * 4 + py) * 4 + px],
+            dst_ref=returned.at[me],
+            send_sem=back_send,
+            recv_sem=back_recv,
+            device_id=(pz, py, px, c),
+            device_id_type=MESH,
+        ).start()
+        return carry
+
+    lax.fori_loop(1, 64, give_back, 0)
+    returned[me] = leaving[me]
+    block_wait(returned, 63, back_recv, twin).wait_recv()
+
+    def total(e, carry):
+        acc = returned[e * 8].astype(F32)
+        for k in range(1, 8):
+            acc += returned[e * 8 + k].astype(F32)
+        summed[pl.ds(pl.multiple_of(e * 24, 8), 24), :] = acc
+        return carry
+
+    lax.fori_loop(0, EXPERTS, total, 0)
+    routed = jnp.dot(
+        mixer[...], summed[...], precision=lax.Precision.HIGHEST, preferred_element_type=F32
+    )
+    for q in range(8):
+        lanes = slice(q * 512, (q + 1) * 512)
+        out[:, lanes] = (after[:, lanes] + routed[q * 8 : (q + 1) * 8, :]).astype(BF16)
+    for swap in swaps:
+        swap.wait_send()
+    block_wait(arrived, 63, out_send, twin).wait_send()
+    block_wait(returned, 63, back_send, twin).wait_send()
+
+
+def experts(blocks, mixer, after, gate_t, up_t, down):
+    vmem = pl.BlockSpec(memory_space=pltpu.VMEM)
+    hbm = pl.BlockSpec(memory_space=pl.ANY)
+    dma = pltpu.SemaphoreType.DMA
+    return pl.pallas_call(
+        expert_kernel,
+        out_shape=jax.ShapeDtypeStruct(after.shape, BF16),
+        in_specs=[vmem, vmem, vmem, hbm, hbm, hbm],
+        out_specs=vmem,
+        scratch_shapes=[
+            pltpu.VMEM((2 * HID, 4096), BF16),
+            pltpu.VMEM((2 * HID, 4096), BF16),
+            pltpu.VMEM((2 * HID, 4096), BF16),
+            pltpu.VMEM((64, 24, 512), BF16),
+            pltpu.VMEM((4, 1536, 128), F32),
+            pltpu.VMEM((192, 4096), BF16),
+            pltpu.VMEM((2, 192, HID), BF16),
+            pltpu.VMEM((64, 24, 512), BF16),
+            pltpu.VMEM((64, 24, 512), BF16),
+            pltpu.VMEM((192, 512), F32),
+            dma((3,)),
+            dma((3,)),
+            dma((3,)),
+            dma,
+            dma,
+            dma,
+            dma,
+        ],
+        compiler_params=pltpu.CompilerParams(
+            collective_id=1, has_side_effects=True, vmem_limit_bytes=56 * 1024 * 1024
+        ),
+        name="experts",
+    )(blocks, mixer, after, gate_t, up_t, down)
 
 
 def attend_local(
@@ -209,31 +421,19 @@
     second = normalize(after_attention, norm_second).astype(jnp.bfloat16)
     owners = owner_table(sequences)
     assign = sequences * TOP
-    group_size = devices // EXPERTS
     weights = jax.nn.softmax(route_scores.astype(jnp.float32), axis=-1)
     matches = slot_tables(route_ids.reshape(1, assign))[0].astype(jnp.float32)
     picker = jnp.einsum("aec,sa->ecs", matches, owners).astype(jnp.bfloat16)
     outbound = jnp.einsum("ecs,sd->ecd", picker, second, preferred_element_type=jnp.float32).astype(
         jnp.bfloat16
     )
-    outbound = jnp.broadcast_to(outbound[:, None], (EXPERTS, group_size, CAP, model_width))
-    outbound = outbound.reshape(devices, CAP, model_width)
-    arrived = lax.all_to_all(outbound, EP_TP, split_axis=0, concat_axis=0, tiled=True)
-    partial_value = expert_rows(
-        arrived.reshape(-1, model_width), expert_gate, expert_up, expert_down
-    )
-    returned = lax.all_to_all(
-        partial_value.reshape(arrived.shape).astype(jnp.bfloat16),
-        EP_TP,
-        split_axis=0,
-        concat_axis=0,
-        tiled=True,
-    ).astype(jnp.float32)
-    summed = jnp.sum(returned.reshape(EXPERTS, group_size, CAP, model_width), axis=1)
+    blocks = outbound.reshape(EXPERTS, CAP * 8, model_width // 8)
     combine_weights = matches * weights.reshape(assign)[:, None, None]
-    token_weights = jnp.einsum("aec,sa->sec", combine_weights, owners)
-    routed = jnp.einsum("sec,ecd->sd", token_weights, summed)
-    layer_out = (after_attention + routed).astype(jnp.bfloat16)
+    token_weights = jnp.einsum("aec,sa->sec", combine_weights, owners, precision="highest")
+    mixer = jnp.einsum("ter,qp->qterp", token_weights, jnp.eye(8, dtype=F32)).reshape(64, 192)
+    layer_out = experts(
+        blocks, mixer, after_attention, expert_gate.T, expert_up.T, expert_down
+    )
     return (layer_out, new_latent, new_rope)
 
 

time: 439 us -> 354 us (0.81)
  Pallas kernels: 0 us -> 65.7 us
  blocking collectives: 142 us -> 84.5 us
  waiting for transfers between devices: 158 us -> 104 us
  matrix products: 42.9 us -> 27.2 us
  local copies, waits for them, and re-layouts: 39.7 us -> 26.5 us
  starting transfers between devices: 20.5 us -> 14.8 us
    pallas_call x0 -> x1, Pallas kernels: none -> 65.7 us  [experts(): pl.pallas_call(expert_kernel, out_shape=jax.ShapeDtypeStruct(after.shape,...]
    all_to_all x1 -> x0, blocking collectives: 57.3 us -> none  [local(): lax.all_to_all(outbound, EP_TP, split_axis=0, concat_axis=0, tiled=True)]
    all_to_all x1 -> x0, waiting for transfers between devices: 51.8 us -> none  [local(): lax.all_to_all(partial_value.reshape(arrived.shape).astype(jnp.bfloat16),...]
    dot_general x3 -> x1, matrix products: 15.7 us -> 0.14 us  [local(): jnp.einsum('aec,sa->sec', combine_weights, owners, precision='highest')]
    convert_element_type x1 -> x0, local copies, waits for them, and re-layouts: 7.08 us -> none  [local(): partial_value.reshape(arrived.shape).astype(jnp.bfloat16)]
    all_to_all x1 -> x0, starting transfers between devices: 5.64 us -> none  [local(): lax.all_to_all(partial_value.reshape(arrived.shape).astype(jnp.bfloat16),...]
    reshape x1 -> x3, local copies, waits for them, and re-layouts: 7.42 us -> 1.9 us  [the longest x2 0.96 us: local(): jnp.einsum('ter,qp->qterp', token_weights, jnp.eye(8, dtype=F32))]
    reduce_sum x1 -> x0, other arithmetic: 4.42 us -> none  [local(): jnp.sum(returned.reshape(EXPERTS, group_size, CAP, model_width), axis=1)]
  transfers between devices with their start and end apart: 5 -> 4, of which waited for: 5 -> 4; matrix products, arithmetic and copies ran while one was open for 0% -> 1% of each run, Pallas kernels for 0% -> 0%
where the time goes in v1:
time: 354 us; the launch traced here: 353 us
  waiting for transfers between devices  104 us (29%)
  blocking collectives  84.5 us (24%)
  Pallas kernels  65.7 us (19%)
  matrix products  27.2 us (8%)
  local copies, waits for them, and re-layouts  26.5 us (7%)
  other arithmetic  15.4 us (4%)
  starting transfers between devices  14.8 us (4%)
  between operations  14.5 us (4%)
    pallas_call x1, Pallas kernels, experts(): pl.pallas_call(expert_kernel, out_shape=jax.ShapeDtypeStruct(after.shape,...  65.7 us
    all_gather x1, waiting for transfers between devices, local(): lax.all_gather(values, EP_TP, axis=0, tiled=True)  64.4 us
    all_to_all x1, blocking collectives, sum_by_axis(): lax.all_to_all(nearer, far, split_axis=0, concat_axis=0, tiled=True)  46.3 us
    all_to_all x1, blocking collectives, local(): lax.all_to_all(normed, EP_TP, split_axis=1, concat_axis=0, tiled=True)  20.9 us
    all_to_all x1, waiting for transfers between devices, sent_to_all(): lax.all_to_all(jnp.broadcast_to(shard[None], (peers, *shard.shape)), axis...  17.4 us
    all_to_all x1, waiting for transfers between devices, local(): lax.all_to_all(columns, EP_TP, split_axis=0, concat_axis=1, tiled=True)  13.6 us
    all_to_all x1, blocking collectives, sent_and_summed(): lax.all_to_all(parts, axis, split_axis=0, concat_axis=0, tiled=True)  10.4 us
    all_to_all x1, waiting for transfers between devices, local(): lax.all_to_all(output_cols, EP_TP, split_axis=0, concat_axis=1, tiled=True)  8.91 us
  transfers between devices with their start and end apart: 4, of which 4 were waited for; matrix products, arithmetic and copies ran while one was open for 1% of the time, Pallas kernels for 0%

profile of v1, /device:TPU:1, one launch (start us, length us, event | category | flops | bytes accessed | tf_op | source)
XLA Modules:
  0.0 353.0 jit_solution(9471026213397481040)
XLA Ops:
  7.2 1.1 fusion.20
  8.3 0.9 fusion.22
  9.2 0.2 all_to_all.46
  9.4 0.2 copy.119
  9.6 0.2 reshape.352
  9.8 20.9 %all_to_all.65 = bf16[128,2,128]{2,1,0:T(2,128)(2,1)S(1)} all-to-all(bf16[128,2,128]{2,1,0:T(2,128)(2,1)S(1)} %reshape.352), channel_id=1, replica_groups=mesh['ep_0'=4,'ep_1'=4,'ep_2'=4,'tp'=2] {'ep_0','ep_1','ep_2','tp'}, dimensions={0} | all-to-all | bytes 131072 | tf_op jit(solution)/shard_map/all_to_all | solution.py:375
  30.7 0.2 reshape.353
  30.8 1.6 fusion.17
  32.5 0.5 fusion.15
  32.9 3.2 pad_maximum_fusion
  36.2 6.5 %copy.83 = f32[1024,1536]{1,0:T(8,128)} copy(f32[1024,1536]{0,1:T(8,128)} %pad_maximum_fusion) | data formatting | bytes 12582912 | tf_op jit(solution)/shard_map/concatenate | solution.py:378
  42.7 3.2 copy.84
  45.9 10.4 %all_to_all.66 = f32[2,64,8,1536]{3,2,1,0:T(8,128)} all-to-all(f32[2,64,8,1536]{3,2,1,0:T(8,128)S(1)} %copy.84), channel_id=1, replica_groups=mesh['ep_0'=4,'ep_1'=4,'ep_2'=4,'tp'=2] {'tp'}, dimensions={0} | all-to-all | bytes 12582912 | tf_op jit(solution)/shard_map/all_to_all | solution.py:32
  56.3 5.4 %reduce_sum.83 = f32[64,8,1536]{2,1,0:T(8,128)} reduce(f32[2,64,8,1536]{3,2,1,0:T(8,128)} %all_to_all.66, f32[]{:T(128)} %constant.39.clone.1), dimensions={0}, to_apply=%region_3.0 | reduce | flops 786432 | bytes 9437188 | tf_op jit(solution)/shard_map/reduce_sum | solution.py:33
  61.7 46.3 %all_to_all.67 = f32[64,8,1536]{2,1,0:T(8,128)} all-to-all(f32[64,8,1536]{2,1,0:T(8,128)} %reduce_sum.83), channel_id=1, replica_groups=mesh['ep_0'=4,'ep_1'=4,'ep_2'=4,'tp'=2] {'ep_0','ep_1','ep_2'}, dimensions={0} | all-to-all | bytes 6291456 | tf_op jit(solution)/shard_map/all_to_all | solution.py:40
  108.0 2.1 reduce_sum.84
  110.1 0.1 multiply_reduce_fusion.1
  110.4 1.1 broadcast_in_dim.13
  111.5 5.7 %all-to-all-start.3 = ((bf16[64,8,1024]{2,1,0:T(8,128)(2,1)}), bf16[64,8,1024]{2,1,0:T(8,128)(2,1)S(1)}, u32[]{:S(2)}, u32[]{:S(2)}) async-start(bf16[64,8,1024]{2,1,0:T(8,128)(2,1)} %broadcast_in_dim.13), calls=%async_computation.3 | async-start | bytes 2097152 | tf_op jit(solution)/shard_map/all_to_all | solution.py:46
  117.2 0.2 fusion.70
  117.5 0.1 subtract_convert_fusion.1
  117.9 17.4 %all-to-all-done.3 = bf16[64,8,1024]{2,1,0:T(8,128)(2,1)S(1)} async-done(((bf16[64,8,1024]{2,1,0:T(8,128)(2,1)}), bf16[64,8,1024]{2,1,0:T(8,128)(2,1)S(1)}, u32[]{:S(2)}, u32[]{:S(2)}) %all-to-all-start.3) | async-done | bytes 1048608 | tf_op jit(solution)/shard_map/all_to_all | solution.py:46
  135.2 0.6 copy.85
  135.8 0.3 broadcast_in_dim.14
  136.1 6.9 %all_to_all.68 = bf16[2,64,8,1024]{3,1,2,0:T(8,128)(2,1)S(1)} all-to-all(bf16[2,64,8,1024]{3,1,2,0:T(8,128)(2,1)S(1)} %broadcast_in_dim.14), channel_id=1, replica_groups=mesh['ep_0'=4,'ep_1'=4,'ep_2'=4,'tp'=2] {'tp'}, dimensions={0} | all-to-all | bytes 4194304 | tf_op jit(solution)/shard_map/all_to_all | solution.py:46
  143.0 3.5 copy.86
  146.5 2.8 dot_general.57
  149.3 0.8 convolution_convert_fusion.1
  150.1 0.6 convolution_convert_fusion.3
  150.8 1.2 copy.88
  152.0 3.7 %all-to-all-start.5 = ((bf16[128,8,144]{2,1,0:T(8,128)(2,1)}), bf16[128,8,144]{2,1,0:T(8,128)(2,1)S(1)}, u32[]{:S(2)}, u32[]{:S(2)}) async-start(bf16[128,8,144]{2,1,0:T(8,128)(2,1)} %copy.88), calls=%async_computation.5 | async-start | bytes 1048576 | tf_op jit(solution)/shard_map/all_to_all | solution.py:403
  155.9 13.6 %all-to-all-done.5 = bf16[128,8,144]{2,1,0:T(8,128)(2,1)S(1)} async-done(((bf16[128,8,144]{2,1,0:T(8,128)(2,1)}), bf16[128,8,144]{2,1,0:T(8,128)(2,1)S(1)}, u32[]{:S(2)}, u32[]{:S(2)}) %all-to-all-start.5) | async-done | bytes 294944 | tf_op jit(solution)/shard_map/all_to_all | solution.py:403
  169.5 0.4 copy.89
  169.9 0.2 copy.91
  170.1 0.2 reshape.342
  170.3 0.2 copy.90
  170.5 0.2 reshape.338
  170.7 5.9 %fusion.69 = f32[8,32,1024]{2,1,0:T(8,128)S(1)} fusion(bf16[8,32,512]{2,1,0:T(8,128)(2,1)S(1)} %reshape.338, bf16[8,1024,512]{2,1,0:T(8,128)(2,1)} %param.22), kind=kOutput, calls=%fused_computation.108 | convolution fusion | flops 268435456 | bytes 9699328 | tf_op jit(solution)/shard_map/shl,spl->shp/dot_general | solution.py:323
  176.6 0.2 fusion.28
  176.9 0.2 fusion.38
  177.1 0.5 fusion.66
  177.6 0.3 fusion.11
  177.9 5.2 %fusion.4 = bf16[8,32,512]{2,1,0:T(8,128)(2,1)S(1)} fusion(bf16[8,1024,512]{2,1,0:T(8,128)(2,1)} %param.22, f32[8,32,1024]{2,1,0:T(8,128)S(1)} %get-tuple-element.16, f32[8,32]{1,0:T(8,128)S(1)} %get-tuple-element.10, f32[8,32]{1,0:T(8,128)S(1)} %fusion.59, f32[8,512]{1,0:T(8,128)S(1)} %get-tuple-element.5, f32[8,32]{1,0:T(8,128)S(1)} %get-tuple-element.9), kind=kOutput, calls=%fused_computation.8 | convolution fusion | flops 269615104 | bytes 9718784 | tf_op jit(solution)/shard_map/shp,spl->shl/dot_general | solution.py:338
  183.2 5.1 %fusion.8 = bf16[8,4096]{1,0:T(8,128)(2,1)} fusion(bf16[512,32,128]{2,1,0:T(8,128)(2,1)S(1)} %copy-done.1, bf16[8,32,512]{2,1,0:T(8,128)(2,1)S(1)} %fusion.4), kind=kOutput, calls=%fused_computation.11 | convolution fusion | flops 33587200 | bytes 4521984 | tf_op jit(solution)/shard_map/shl,lhv->shv/dot_general | solution.py:412
  188.8 0.2 select_reduce_fusion
  189.1 0.1 fusion.30
  189.3 0.2 multiply_bitcast_fusion
  189.5 0.2 reshape.341
  189.7 0.7 copy.99.mixer
  190.5 64.4 %all-gather.2.cloned.1.call-done = bf16[1024,4096]{1,0:T(8,128)(2,1)} async-done(((bf16[8,4096]{1,0:T(8,128)(2,1)}), bf16[1024,4096]{1,0:T(8,128)(2,1)}) %all-gather.2.cloned.1.call-update) | async-done | bytes 8388624 | tf_op jit(solution)/shard_map/all_gather | solution.py:415
  254.9 5.9 %convolution_convert_fusion.2 = bf16[1024,32]{0,1:T(8,128)(2,1)S(1)} fusion(bf16[1024,4096]{1,0:T(8,128)(2,1)} %all-gather.2.cloned.1.call-done, bf16[4096,32]{0,1:T(8,128)(2,1)S(1)} %copy-done.6), kind=kOutput, calls=%fused_computation.12 | convolution fusion | flops 268468224 | bytes 8716288 | tf_op jit(solution)/shard_map/dot_general | solution.py:414
  260.8 0.2 copy.94
  261.0 0.8 reshape.354
  261.8 5.4 %all-to-all-start.6 = ((bf16[128,2,128]{2,1,0:T(2,128)(2,1)}), bf16[128,2,128]{2,1,0:T(2,128)(2,1)S(1)}, u32[]{:S(2)}, u32[]{:S(2)}) async-start(bf16[128,2,128]{2,1,0:T(2,128)(2,1)} %reshape.354), calls=%async_computation.6 | async-start | bytes 131072 | tf_op jit(solution)/shard_map/all_to_all | solution.py:419
  267.2 0.7 pad_maximum_fusion.5
  267.9 8.9 %all-to-all-done.6 = bf16[128,2,128]{2,1,0:T(2,128)(2,1)S(1)} async-done(((bf16[128,2,128]{2,1,0:T(2,128)(2,1)}), bf16[128,2,128]{2,1,0:T(2,128)(2,1)S(1)}, u32[]{:S(2)}, u32[]{:S(2)}) %all-to-all-start.6) | async-done | bytes 65568 | tf_op jit(solution)/shard_map/all_to_all | solution.py:419
  276.8 0.2 reshape.355
  277.1 0.2 reshape.343
  277.3 0.1 multiply_reduce_fusion
  277.5 0.3 convolution_convert_fusion
  277.8 0.2 copy.96
  278.0 0.9 reshape.340.blocks
  278.9 65.7 %experts.1 = bf16[8,4096]{1,0:T(8,128)(2,1)} custom-call(bf16[8,24,512]{2,1,0:T(8,128)(2,1)} %reshape.340.blocks, f32[64,192]{1,0:T(8,128)} %copy.99.mixer, f32[8,4096]{1,0:T(8,128)} %copy-done.2, bf16[448,4096]{1,0:T(8,128)(2,1)} %bitcast.77, bf16[448,4096]{1,0:T(8,128)(2,1)} %bitcast.78, bf16[448,4096]{1,0:T(8,128)(2,1)} %down_hbm.1), custom_call_target="tpu_custom_call" | custom-call | tf_op jit(solution)/shard_map/experts/pallas_call | solution.py:287
  344.6 1.5 copy.121
  (68 shorter events, 1.5 us)
Async XLA Ops:
  7.2 169.9 %copy-start = (bf16[8,1024,64]{1,2,0:T(8,128)(2,1)S(1)}, bf16[8,1024,64]{1,2,0:T(8,128)(2,1)}, u32[]{:S(2)}) copy-start(bf16[8,1024,64]{1,2,0:T(8,128)(2,1)} %param.23) | copy-start | bytes 3145732
  7.2 25.3 %copy-start.7 = (bf16[32,512]{1,0:T(8,128)(2,1)S(1)}, bf16[32,512]{1,0:T(8,128)(2,1)}, u32[]{:S(2)}) copy-start(bf16[32,512]{1,0:T(8,128)(2,1)} %param.31) | copy-start | bytes 98308
  61.7 48.6 %copy-start.11 = (f32[1024]{0:T(1024)S(1)}, f32[1024]{0:T(1024)}, u32[]{:S(2)}) copy-start(f32[1024]{0:T(1024)} %param.28) | copy-start | bytes 12292
  108.0 9.2 %copy-start.14 = (s32[8]{0:T(128)S(1)}, s32[8]{0:T(128)}, u32[]{:S(2)}) copy-start(s32[8]{0:T(128)} %param.21) | copy-start | bytes 100
  108.0 9.2 %copy-start.4 = (bf16[4096,64]{0,1:T(8,128)(2,1)S(1)}, bf16[4096,64]{0,1:T(8,128)(2,1)}, u32[]{:S(2)}) copy-start(bf16[4096,64]{0,1:T(8,128)(2,1)} %param.32) | copy-start | bytes 1572868
  111.5 23.8 %all-to-all-start.3 = ((bf16[64,8,1024]{2,1,0:T(8,128)(2,1)}), bf16[64,8,1024]{2,1,0:T(8,128)(2,1)S(1)}, u32[]{:S(2)}, u32[]{:S(2)}) async-start(bf16[64,8,1024]{2,1,0:T(8,128)(2,1)} %broadcast_in_dim.13), calls=%async_computation.3 | async-start | bytes 2097152 | tf_op jit(solution)/shard_map/all_to_all | solution.py:46
  143.0 6.3 %copy-start.5 = (bf16[1024,128]{1,0:T(8,128)(2,1)S(1)}, bf16[1024,128]{1,0:T(8,128)(2,1)}, u32[]{:S(2)}) copy-start(bf16[1024,128]{1,0:T(8,128)(2,1)} %param.33) | copy-start | bytes 786436
  146.5 3.6 %copy-start.8 = (bf16[1024,16]{0,1:T(8,128)(2,1)S(1)}, bf16[1024,16]{0,1:T(8,128)(2,1)}, u32[]{:S(2)}) copy-start(bf16[1024,16]{0,1:T(8,128)(2,1)} %param.34) | copy-start | bytes 98308
  149.3 6.5 %copy-start.12 = (f32[512]{0:T(512)S(1)}, f32[512]{0:T(512)}, u32[]{:S(2)}) copy-start(f32[512]{0:T(512)} %param.29) | copy-start | bytes 6148
  152.0 17.5 %all-to-all-start.5 = ((bf16[128,8,144]{2,1,0:T(8,128)(2,1)}), bf16[128,8,144]{2,1,0:T(8,128)(2,1)S(1)}, u32[]{:S(2)}, u32[]{:S(2)}) async-start(bf16[128,8,144]{2,1,0:T(8,128)(2,1)} %copy.88), calls=%async_computation.5 | async-start | bytes 1048576 | tf_op jit(solution)/shard_map/all_to_all | solution.py:403
  155.7 99.1 %all-gather.2.cloned.1.call-start = ((), (), s32[]{:S(2)}) async-start(), calls=%async_computation.7 | async-start | bytes 8454144 | tf_op jit(solution)/shard_map/all_gather | solution.py:415
  155.9 20.7 %copy-start.10 = (bf16[8,512]{1,0:T(8,128)(2,1)}, bf16[8,512]{1,0:T(8,128)(2,1)S(1)}, u32[]{:S(2)}) copy-start(bf16[8,512]{1,0:T(8,128)(2,1)S(1)} %get-tuple-element.21) | copy-start | bytes 24580
  177.9 5.2 %copy-start.1 = (bf16[512,32,128]{2,1,0:T(8,128)(2,1)S(1)}, bf16[512,32,128]{2,1,0:T(8,128)(2,1)}, u32[]{:S(2)}) copy-start(bf16[512,32,128]{2,1,0:T(8,128)(2,1)} %param.35) | copy-start | bytes 12582916
  183.1 5.2 %copy-start.13 = (s32[8,2]{0,1:T(2,128)S(1)}, s32[8,2]{0,1:T(2,128)}, u32[]{:S(2)}) copy-start(s32[8,2]{0,1:T(2,128)} %param.24) | copy-start | bytes 196
  183.1 5.4 %copy-start.15 = (bf16[8,2]{0,1:T(2,128)(2,1)S(1)}, bf16[8,2]{0,1:T(2,128)(2,1)}, u32[]{:S(2)}) copy-start(bf16[8,2]{0,1:T(2,128)(2,1)} %param.25) | copy-start | bytes 100
  183.2 71.7 %copy-start.6 = (bf16[4096,32]{0,1:T(8,128)(2,1)S(1)}, bf16[4096,32]{0,1:T(8,128)(2,1)}, u32[]{:S(2)}) copy-start(bf16[4096,32]{0,1:T(8,128)(2,1)} %param.36) | copy-start | bytes 786436
  190.5 86.9 %copy-start.3 = (bf16[8,4096]{1,0:T(8,128)(2,1)S(1)}, bf16[8,4096]{1,0:T(8,128)(2,1)}, u32[]{:S(2)}) copy-start(bf16[8,4096]{1,0:T(8,128)(2,1)} %param.20) | copy-start | bytes 196612
  190.5 87.0 %copy-start.9 = (f32[4096]{0:T(1024)S(1)}, f32[4096]{0:T(1024)}, u32[]{:S(2)}) copy-start(f32[4096]{0:T(1024)} %param.27) | copy-start | bytes 49156
  261.8 14.9 %all-to-all-start.6 = ((bf16[128,2,128]{2,1,0:T(2,128)(2,1)}), bf16[128,2,128]{2,1,0:T(2,128)(2,1)S(1)}, u32[]{:S(2)}, u32[]{:S(2)}) async-start(bf16[128,2,128]{2,1,0:T(2,128)(2,1)} %reshape.354), calls=%async_computation.6 | async-start | bytes 131072 | tf_op jit(solution)/shard_map/all_to_all | solution.py:419
  277.5 1.5 copy-start.2
Sparse Core Ops, SparseCore 0:
  188.4 66.3 all-gather.1
